TPU v7x, 256 devices: a 4x2x16 block of a 4x16x16 slice. The times are simulated.
256 devices in a mesh: grp: 2 (over y), fs: 16 (over z), tp: 8 (over x, core).
Axes of the slice: x: 4, y: 2, z: 16, core: 2. Of those that a mesh axis runs over, the one named last changes fastest.
The devices are a block of a 4x16x16 slice.
Arguments:
- tokens: bfloat16 [32768, 2048], P(('grp', 'fs'), 'tp'), parts along dimension 0, may hold values from -6 to 6
- mixer_gain: float32 [2048], replicated, may hold values from 0.1 to 1.9
- branch_weight: float32 [2048, 1024], P('fs', 'tp'), may hold values from -0.125 to 0.125
- gelu_weight: float32 [2048, 1024], P('fs', 'tp'), may hold values from -0.125 to 0.125
- branch_scale: float32 [16, 64], P('fs', 'tp'), may hold values from 0.5 to 2
- gelu_scale: float32 [16, 64], P('fs', 'tp'), may hold values from 0.5 to 2
- branch_taps: float32 [4, 1024], P(None, 'tp'), may hold values from -3 to 3
- recur_gate: bfloat16 [16, 64, 64], P('tp'), may hold values from -0.75 to 0.75
- input_gate: bfloat16 [16, 64, 64], P('tp'), may hold values from -0.75 to 0.75
- decay_param: float32 [1024], P('tp'), may hold values from 4 to 7
- out_weight: float32 [1024, 2048], P('tp', 'fs'), may hold values from -0.5 to 0.5
- out_scale: float32 [16, 128], P('fs'), may hold values from 0.5 to 2
- ffn_gain: float32 [2048], replicated, may hold values from 0.1 to 1.9
- upgate_weight: float32 [2048, 5632], P('fs', 'tp'), may hold values from -0.125 to 0.125
- upval_weight: float32 [2048, 5632], P('fs', 'tp'), may hold values from -0.125 to 0.125
- upgate_scale: float32 [16, 352], P('fs', 'tp'), may hold values from 0.5 to 2
- upval_scale: float32 [16, 352], P('fs', 'tp'), may hold values from 0.5 to 2
- upgate_taps: float32 [3, 5632], P(None, 'tp'), may hold values from -3 to 3
- upval_taps: float32 [3, 5632], P(None, 'tp'), may hold values from -3 to 3
- down_weight: float32 [5632, 2048], P('tp', 'fs'), may hold values from -0.15625 to 0.15625
- down_scale: float32 [16, 128], P('fs'), may hold values from 0.5 to 2
Outputs:
- layer_out: bfloat16 [32768, 2048], P(('grp', 'fs'), 'tp'), parts along dimension 0
There are 2 independent parts, one for each index of `grp`. A program takes and returns all parts, laid end to end along the dimension named above; an argument that names none is the same for every part. Nothing has to cross between parts.
All inputs are finite; a program needn't handle non-finite values.
Results may differ from a plain program's by a relative error of at most 0.024.
Values may be sent and summed in bfloat16 or wider, within the bound.
No kernel may reach another device: no remote copies, remote signals or barrier semaphores. Data moves between devices by JAX's collectives and lax.ppermute only.
A program may use at most 128 MiB of HBM per device.

v0:
```python
import jax
import jax.numpy as jnp
from jax import lax
from jax.sharding import PartitionSpec as P

SEQ_LEN = 512


def side_by_side(arrays, axis, dim, along):
    both = jnp.concatenate(arrays, axis=along)
    filled, at, outs = (lax.all_gather(both, axis, axis=dim, tiled=True), 0, [])
    for a in arrays:
        outs.append(lax.slice_in_dim(filled, at, at + a.shape[along], axis=along))
        at += a.shape[along]
    return tuple(outs)


def copy_for_each(value, axis):
    size = lax.axis_size(axis)
    return lax.all_to_all(
        jnp.broadcast_to(value[None], (size, *value.shape)), axis, 0, 0, tiled=True
    )


def in_order(blocks, dim):
    lengths = list(blocks.shape[1:])
    lengths[dim] *= blocks.shape[0]
    return jnp.moveaxis(blocks, 0, dim).reshape(lengths)


def gather_directly(value, axis, dim):
    blocks = copy_for_each(value, axis)
    return in_order(blocks, dim)


def rms_rows(values_in, norm_gain):
    values = values_in.astype(jnp.float32)
    inverse = lax.rsqrt(jnp.mean(values * values, axis=-1, keepdims=True) + 1e-06)
    return (values * inverse * norm_gain).astype(jnp.bfloat16)


def expand_scale(gathered):
    return gathered.T.reshape(-1)


def causal_mix(values, filter_taps, seq_len):
    columns = values.shape[-1]
    grouped = values.reshape(-1, seq_len, columns)
    tap_count = filter_taps.shape[0]
    padded = jnp.pad(grouped, ((0, 0), (tap_count - 1, 0), (0, 0)))
    totals = padded[:, 0:seq_len] * filter_taps[0]
    for k in range(1, tap_count):
        totals = totals + padded[:, k : k + seq_len] * filter_taps[k]
    return totals.reshape(-1, columns)


def combine_pairs(earlier, later):
    return (earlier[0] * later[0], later[0] * earlier[1] + later[1])


def run_scan(factors, inputs, seq_len):
    columns = factors.shape[-1]
    pair = (factors.reshape(-1, seq_len, columns), inputs.reshape(-1, seq_len, columns))
    _, states = lax.associative_scan(combine_pairs, pair, axis=1)
    return states.reshape(-1, columns)


def add_rows(left, weight_piece):
    return jnp.dot(left, weight_piece, preferred_element_type=jnp.float32)


def per_device(
    tokens,
    mixer_gain,
    branch_weight,
    gelu_weight,
    branch_scale,
    gelu_scale,
    branch_taps,
    recur_gate,
    input_gate,
    decay_param,
    out_weight,
    out_scale,
    ffn_gain,
    upgate_weight,
    upval_weight,
    upgate_scale,
    upval_scale,
    upgate_taps,
    upval_taps,
    down_weight,
    down_scale,
):
    scale_list = side_by_side(
        (branch_scale, gelu_scale, out_scale, upgate_scale, upval_scale, down_scale), "fs", 0, 1
    )
    mixer_scales = scale_list[:3]
    ffn_scales = scale_list[3:]
    gathered = gather_directly(tokens, "tp", 1)
    normed = rms_rows(gathered, mixer_gain)
    pieces = side_by_side(
        (branch_weight.astype(jnp.bfloat16), gelu_weight.astype(jnp.bfloat16)), "fs", 0, 1
    )
    branch = add_rows(normed, pieces[0])
    gelu_in = add_rows(normed, pieces[1])
    branch = branch * expand_scale(mixer_scales[0])
    gelu_in = gelu_in * expand_scale(mixer_scales[1])
    convolved = causal_mix(branch, branch_taps, SEQ_LEN).astype(jnp.bfloat16)
    local_blocks = recur_gate.shape[0]
    blocks = convolved.reshape(convolved.shape[0], local_blocks, recur_gate.shape[1])
    channels = convolved.shape[1]
    recur = jax.nn.sigmoid(
        jnp.einsum("rnc,ncd->rnd", blocks, recur_gate, preferred_element_type=jnp.float32).reshape(
            -1, channels
        )
    )
    input_rate = jax.nn.sigmoid(
        jnp.einsum("rnc,ncd->rnd", blocks, input_gate, preferred_element_type=jnp.float32).reshape(
            -1, channels
        )
    )
    log_decay = -8.0 * recur * jax.nn.softplus(-decay_param)
    decay_rate = jnp.exp(log_decay)
    driven = jnp.sqrt(-jnp.expm1(2.0 * log_decay)) * input_rate * convolved.astype(jnp.float32)
    states = run_scan(decay_rate, driven, SEQ_LEN)
    gated_state = (states * jax.nn.gelu(gelu_in)).astype(jnp.bfloat16)
    out_cols = expand_scale(mixer_scales[2])
    tp_count = lax.axis_size("tp")
    feature_width = tokens.shape[1]
    whole_state = gather_directly(gated_state, "tp", 1)
    row_block = gather_directly(out_weight.astype(jnp.bfloat16), "fs", 1)
    own_columns = lax.all_to_all(row_block, "tp", split_axis=1, concat_axis=0, tiled=True)
    first_feature = lax.axis_index("tp") * feature_width
    own_scales = lax.dynamic_slice_in_dim(out_cols, first_feature, feature_width, 0)
    block_rows = whole_state.shape[1] // tp_count
    mixer_sum = jnp.zeros((whole_state.shape[0], feature_width), jnp.float32)
    for index in range(tp_count):
        partial_value = (
            jnp.dot(
                whole_state[:, index * block_rows : (index + 1) * block_rows],
                own_columns[index * block_rows : (index + 1) * block_rows],
                preferred_element_type=jnp.float32,
            )
            * own_scales
        )
        mixer_sum = mixer_sum + partial_value.astype(jnp.bfloat16).astype(jnp.float32)
    hidden_state = (tokens.astype(jnp.float32) + mixer_sum).astype(jnp.bfloat16)
    gathered_ffn = gather_directly(hidden_state, "tp", 1)
    normed_ffn = rms_rows(gathered_ffn, ffn_gain)
    upgate_bf = upgate_weight.astype(jnp.bfloat16)
    upval_bf = upval_weight.astype(jnp.bfloat16)
    gate_full, value_full = side_by_side((upgate_bf, upval_bf), "fs", 0, 1)
    up_gate = jnp.dot(normed_ffn, gate_full, preferred_element_type=jnp.float32)
    up_val = jnp.dot(normed_ffn, value_full, preferred_element_type=jnp.float32)
    up_gate = up_gate * expand_scale(ffn_scales[0])
    up_val = up_val * expand_scale(ffn_scales[1])
    conv_gate = causal_mix(up_gate, upgate_taps, SEQ_LEN)
    conv_val = causal_mix(up_val, upval_taps, SEQ_LEN)
    ffn_hidden = (jax.nn.silu(conv_gate) * conv_val).astype(jnp.bfloat16)
    down_cols = expand_scale(ffn_scales[2])
    ffn_terms = (
        jnp.dot(
            ffn_hidden,
            lax.all_gather(down_weight.astype(jnp.bfloat16), "fs", axis=1, tiled=True),
            preferred_element_type=jnp.float32,
        )
        * down_cols
    ).astype(jnp.bfloat16)
    ffn_sum = lax.psum_scatter(ffn_terms, "tp", scatter_dimension=1, tiled=True).astype(jnp.float32)
    return (hidden_state.astype(jnp.float32) + ffn_sum).astype(jnp.bfloat16)


def solution(mesh):
    in_specs = (
        P(("grp", "fs"), "tp"),
        P(),
        P("fs", "tp"),
        P("fs", "tp"),
        P("fs", "tp"),
        P("fs", "tp"),
        P(None, "tp"),
        P("tp", None, None),
        P("tp", None, None),
        P("tp"),
        P("tp", "fs"),
        P("fs", None),
        P(),
        P("fs", "tp"),
        P("fs", "tp"),
        P("fs", "tp"),
        P("fs", "tp"),
        P(None, "tp"),
        P(None, "tp"),
        P("tp", "fs"),
        P("fs", None),
    )
    out_specs = P(("grp", "fs"), "tp")
    return jax.shard_map(
        per_device, mesh=mesh, in_specs=in_specs, out_specs=out_specs, check_vma=False
    )
```

profile of v0, /device:TPU:40, one launch (start us, length us, event | category | flops | bytes accessed | tf_op | source)
XLA Modules:
  0.0 379.5 jit_solution(1736366279344310207)
XLA Ops:
  6.6 0.9 convert_element_type.151
  7.5 0.9 broadcast_in_dim.10
  8.4 24.0 %all-to-all-start.2 = ((bf16[16,128,128]{1,2,0:T(8,128)(2,1)}), bf16[16,128,128]{1,2,0:T(8,128)(2,1)}, u32[]{:S(2)}, u32[]{:S(2)}) async-start(bf16[16,128,128]{1,2,0:T(8,128)(2,1)} %broadcast_in_dim.10), calls=%async_computation.2 | async-start | bytes 1048576 | tf_op jit(solution)/shard_map/all_to_all | solution.py:20
  32.4 1.2 copy.50
  33.7 27.7 %all-to-all-done.2 = bf16[16,128,128]{1,2,0:T(8,128)(2,1)} async-done(((bf16[16,128,128]{1,2,0:T(8,128)(2,1)}), bf16[16,128,128]{1,2,0:T(8,128)(2,1)}, u32[]{:S(2)}, u32[]{:S(2)}) %all-to-all-start.2) | async-done | bytes 524320 | tf_op jit(solution)/shard_map/all_to_all | solution.py:20
  61.4 2.6 broadcast_in_dim.8
  64.1 4.9 %all-to-all-start = ((bf16[8,1024,256]{1,2,0:T(8,128)(2,1)}), bf16[8,1024,256]{1,2,0:T(8,128)(2,1)}, u32[]{:S(2)}, u32[]{:S(2)}) async-start(bf16[8,1024,256]{1,2,0:T(8,128)(2,1)} %broadcast_in_dim.8), calls=%async_computation | async-start | bytes 8388608 | tf_op jit(solution)/shard_map/all_to_all | solution.py:20
  69.2 0.6 pad_maximum_fusion.3
  70.0 0.8 pad_maximum_fusion
  71.0 30.5 %all-gather = f32[16,1,360]{2,1,0:T(1,128)S(1)} all-gather(f32[1,1,360]{2,1,0:T(1,128)S(1)} %bitcast.154), channel_id=1, replica_groups=mesh['grp'=2,'fs'=16,'tp'=8] {'fs'}, dimensions={0}, use_global_device_ids=true | all-gather | bytes 24480 | tf_op jit(solution)/shard_map/all_gather | solution.py:11
  102.0 16.7 %all-to-all-done = bf16[8,1024,256]{1,2,0:T(8,128)(2,1)} async-done(((bf16[8,1024,256]{1,2,0:T(8,128)(2,1)}), bf16[8,1024,256]{1,2,0:T(8,128)(2,1)}, u32[]{:S(2)}, u32[]{:S(2)}) %all-to-all-start) | async-done | bytes 4194336 | tf_op jit(solution)/shard_map/all_to_all | solution.py:20
  118.6 3.9 %all-to-all-start.3 = ((bf16[128,8,256]{0,2,1:T(8,128)(2,1)}), bf16[128,8,256]{0,2,1:T(8,128)(2,1)S(1)}, u32[]{:S(2)}, u32[]{:S(2)}) async-start(bf16[128,8,256]{0,2,1:T(8,128)(2,1)} %bitcast.16), calls=%async_computation.3 | async-start | bytes 1048576 | tf_op jit(solution)/shard_map/all_to_all | solution.py:133
  122.5 3.1 multiply_reduce_fusion.1
  125.6 4.2 %fusion.3 = bf16[1024,2048]{0,1:T(8,128)(2,1)} fusion(f32[2048]{0:T(1024)S(1)} %copy-done.10, f32[1024]{0:T(1024)S(1)} %add_rsqrt_fusion.1, bf16[8,1024,256]{1,2,0:T(8,128)(2,1)} %all-to-all-done), kind=kLoop, calls=%fused_computation.5 | loop fusion | flops 8388608 | bytes 8400896 | tf_op jit(solution)/shard_map/convert_element_type | solution.py:39
  129.8 6.7 %all-gather.5.cloned.1.call-done = bf16[2048,256]{1,0:T(8,128)(2,1)} async-done(((bf16[128,256]{1,0:T(8,128)(2,1)}), bf16[2048,256]{1,0:T(8,128)(2,1)}) %all-gather.5.cloned.1.call-update) | async-done | bytes 1048592 | tf_op jit(solution)/shard_map/all_gather | solution.py:11
  136.5 3.6 convolution_multiply_fusion.9
  140.7 0.3 fusion.55
  141.1 0.4 div.27
  141.8 0.3 fusion.51
  142.1 0.4 div.29
  142.8 0.6 multiply_exponential_fusion
  146.6 0.8 copy-done.22
  147.4 3.5 fusion.64
  151.1 1.6 broadcast_in_dim.9
  152.7 4.3 %all-to-all-start.1 = ((bf16[8,1024,128]{1,2,0:T(8,128)(2,1)}), bf16[8,1024,128]{1,2,0:T(8,128)(2,1)S(1)}, u32[]{:S(2)}, u32[]{:S(2)}) async-start(bf16[8,1024,128]{1,2,0:T(8,128)(2,1)} %broadcast_in_dim.9), calls=%async_computation.1 | async-start | bytes 4194304 | tf_op jit(solution)/shard_map/all_to_all | solution.py:20
  157.3 26.8 %all-to-all-done.1 = bf16[8,1024,128]{1,2,0:T(8,128)(2,1)S(1)} async-done(((bf16[8,1024,128]{1,2,0:T(8,128)(2,1)}), bf16[8,1024,128]{1,2,0:T(8,128)(2,1)S(1)}, u32[]{:S(2)}, u32[]{:S(2)}) %all-to-all-start.1) | async-done | bytes 2097184 | tf_op jit(solution)/shard_map/all_to_all | solution.py:20
  184.5 0.3 fusion.36
  185.2 0.3 fusion.40
  186.5 0.6 fusion.47
  187.3 2.5 broadcast_in_dim.11
  189.9 4.9 %all-to-all-start.4 = ((bf16[8,1024,256]{1,2,0:T(8,128)(2,1)}), bf16[8,1024,256]{1,2,0:T(8,128)(2,1)}, u32[]{:S(2)}, u32[]{:S(2)}) async-start(bf16[8,1024,256]{1,2,0:T(8,128)(2,1)} %broadcast_in_dim.11), calls=%async_computation.4 | async-start | bytes 8388608 | tf_op jit(solution)/shard_map/all_to_all | solution.py:20
  194.8 0.7 convert_element_type.178
  196.4 47.9 %all-to-all-done.4 = bf16[8,1024,256]{1,2,0:T(8,128)(2,1)} async-done(((bf16[8,1024,256]{1,2,0:T(8,128)(2,1)}), bf16[8,1024,256]{1,2,0:T(8,128)(2,1)}, u32[]{:S(2)}, u32[]{:S(2)}) %all-to-all-start.4) | async-done | bytes 4194336 | tf_op jit(solution)/shard_map/all_to_all | solution.py:20
  244.3 3.1 multiply_reduce_fusion
  247.4 4.1 %fusion.1 = bf16[1024,2048]{0,1:T(8,128)(2,1)} fusion(f32[2048]{0:T(1024)S(1)} %copy-done.11, f32[1024]{0:T(1024)S(1)} %add_rsqrt_fusion, bf16[8,1024,256]{1,2,0:T(8,128)(2,1)} %all-to-all-done.4), kind=kLoop, calls=%fused_computation.2 | loop fusion | flops 8388608 | bytes 8400896 | tf_op jit(solution)/shard_map/convert_element_type | solution.py:39
  251.5 7.9 %fusion.16 = f32[1024,704]{0,1:T(8,128)} fusion(bf16[1024,2048]{0,1:T(8,128)(2,1)} %fusion.1, bf16[2048,1408]{0,1:T(8,128)(2,1)} %all-gather.7.cloned.1.call-done, f32[704]{0:T(1024)S(1)} %mul.461), kind=kOutput, calls=%fused_computation.26 | convolution fusion | flops 2953510912 | bytes 9964288 | tf_op jit(solution)/shard_map/dot_general | solution.py:154
  259.4 4.0 %reshape.117 = f32[2,512,704]{1,0,2:T(2,128)S(1)} reshape(f32[1024,704]{0,1:T(8,128)} %fusion.16) | data formatting | bytes 5767168 | tf_op jit(solution)/shard_map/reshape | solution.py:48
  263.4 9.4 %fusion.6 = f32[2,512,704]{1,0,2:T(2,128)S(1)} fusion(f32[2,512,704]{1,0,2:T(2,128)S(1)} %reshape.117, f32[704]{0:T(1024)S(1)} %get-tuple-element.6, f32[704]{0:T(1024)S(1)} %get-tuple-element.7, f32[704]{0:T(1024)S(1)} %get-tuple-element.5), kind=kLoop, calls=%fused_computation.15 | loop fusion | flops 3604480 | bytes 5775616 | tf_op jit(solution)/shard_map/add | solution.py:53
  272.8 2.3 copy.76
  275.1 0.9 copy-done.2
  276.0 4.7 %fusion.19 = f32[1024,704]{0,1:T(8,128)} fusion(bf16[1024,2048]{0,1:T(8,128)(2,1)S(1)} %copy-done.2, bf16[2048,1408]{0,1:T(8,128)(2,1)S(1)} %copy-done.21, f32[704]{0:T(1024)S(1)} %mul.474), kind=kOutput, calls=%fused_computation.27 | convolution fusion | flops 2953510912 | bytes 9965568 | tf_op jit(solution)/shard_map/dot_general | solution.py:155
  280.8 4.0 %reshape.119 = f32[2,512,704]{1,0,2:T(2,128)S(1)} reshape(f32[1024,704]{0,1:T(8,128)} %fusion.19) | data formatting | bytes 5767168 | tf_op jit(solution)/shard_map/reshape | solution.py:48
  284.7 9.7 %fusion.10 = f32[2,512,704]{1,0,2:T(2,128)S(1)} fusion(f32[2,512,704]{1,0,2:T(2,128)S(1)} %reshape.119, f32[704]{0:T(1024)S(1)} %get-tuple-element.9, f32[704]{0:T(1024)S(1)} %get-tuple-element.10, f32[704]{0:T(1024)S(1)} %get-tuple-element.8), kind=kLoop, calls=%fused_computation.19 | loop fusion | flops 3604480 | bytes 5775616 | tf_op jit(solution)/shard_map/add | solution.py:53
  294.4 2.3 copy.77
  296.7 25.5 %all-gather.9.cloned.1.call-done = bf16[704,2048]{1,0:T(8,128)(2,1)} async-done(((bf16[704,128]{1,0:T(8,128)(2,1)}), bf16[704,2048]{1,0:T(8,128)(2,1)}) %all-gather.9.cloned.1.call-update) | async-done | bytes 2883600 | tf_op jit(solution)/shard_map/all_gather | solution.py:165
  322.2 8.2 %multiply_convert_fusion = bf16[1024,2048]{1,0:T(8,128)(2,1)} fusion(bf16[704,2048]{1,0:T(8,128)(2,1)} %all-gather.9.cloned.1.call-done, f32[2048]{0:T(1024)S(1)} %mul.487, f32[1024,704]{0,1:T(8,128)} %bitcast.129, f32[1024,704]{0,1:T(8,128)S(1)} %bitcast.128), kind=kOutput, calls=%fused_computation.6 | convolution fusion | flops 2961309696 | bytes 12853248 | tf_op jit(solution)/shard_map/dot_general | solution.py:163
  330.5 40.5 %reduce-scatter.2.cloned.1.call-done = bf16[1024,256]{1,0:T(8,128)(2,1)} async-done(((bf16[1024,2048]{1,0:T(8,128)(2,1)}), bf16[1024,256]{1,0:T(8,128)(2,1)}) %reduce-scatter.2.cloned.1.call-update) | async-done | bytes 524304 | tf_op jit(solution)/shard_map/reduce_scatter | solution.py:170
  371.0 2.0 add_convert_fusion
  (202 shorter events, 7.9 us)
Async XLA Ops:
  6.5 134.2 %copy-start = (bf16[2,64,64]{2,1,0:T(8,128)(2,1)S(1)}, bf16[2,64,64]{2,1,0:T(8,128)(2,1)}, u32[]{:S(2)}) copy-start(bf16[2,64,64]{2,1,0:T(8,128)(2,1)} %param.28) | copy-start | bytes 49156
  8.4 53.0 %all-to-all-start.2 = ((bf16[16,128,128]{1,2,0:T(8,128)(2,1)}), bf16[16,128,128]{1,2,0:T(8,128)(2,1)}, u32[]{:S(2)}, u32[]{:S(2)}) async-start(bf16[16,128,128]{1,2,0:T(8,128)(2,1)} %broadcast_in_dim.10), calls=%async_computation.2 | async-start | bytes 1048576 | tf_op jit(solution)/shard_map/all_to_all | solution.py:20
  64.0 5.1 %copy-start.8 = (f32[128,128]{1,0:T(8,128)S(1)}, f32[128,128]{1,0:T(8,128)}, u32[]{:S(2)}) copy-start(f32[128,128]{1,0:T(8,128)} %param.23) | copy-start | bytes 196612
  64.0 5.1 %copy-start.9 = (f32[128,128]{1,0:T(8,128)S(1)}, f32[128,128]{1,0:T(8,128)}, u32[]{:S(2)}) copy-start(f32[128,128]{1,0:T(8,128)} %param.24) | copy-start | bytes 196612
  64.0 5.9 %copy-start.5 = (f32[128,704]{0,1:T(8,128)S(1)}, f32[128,704]{0,1:T(8,128)}, u32[]{:S(2)}) copy-start(f32[128,704]{0,1:T(8,128)} %param.34) | copy-start | bytes 1081348
  64.0 5.9 %copy-start.6 = (f32[128,704]{0,1:T(8,128)S(1)}, f32[128,704]{0,1:T(8,128)}, u32[]{:S(2)}) copy-start(f32[128,704]{0,1:T(8,128)} %param.35) | copy-start | bytes 1081348
  64.0 6.8 %copy-start.15 = (f32[1,8]{1,0:T(1,128)S(1)}, f32[1,8]{1,0:T(1,128)}, u32[]{:S(2)}) copy-start(f32[1,8]{1,0:T(1,128)} %param.25) | copy-start | bytes 100
  64.1 6.8 %copy-start.16 = (f32[1,8]{1,0:T(1,128)S(1)}, f32[1,8]{1,0:T(1,128)}, u32[]{:S(2)}) copy-start(f32[1,8]{1,0:T(1,128)} %param.26) | copy-start | bytes 100
  64.1 6.8 %copy-start.17 = (f32[1,128]{1,0:T(1,128)S(1)}, f32[1,128]{1,0:T(1,128)}, u32[]{:S(2)}) copy-start(f32[1,128]{1,0:T(1,128)} %param.32) | copy-start | bytes 1540
  64.1 6.8 %copy-start.18 = (f32[1,44]{1,0:T(1,128)S(1)}, f32[1,44]{1,0:T(1,128)}, u32[]{:S(2)}) copy-start(f32[1,44]{1,0:T(1,128)} %param.36) | copy-start | bytes 532
  64.1 6.8 %copy-start.19 = (f32[1,44]{1,0:T(1,128)S(1)}, f32[1,44]{1,0:T(1,128)}, u32[]{:S(2)}) copy-start(f32[1,44]{1,0:T(1,128)} %param.37) | copy-start | bytes 532
  64.1 6.8 %copy-start.20 = (f32[1,128]{1,0:T(1,128)S(1)}, f32[1,128]{1,0:T(1,128)}, u32[]{:S(2)}) copy-start(f32[1,128]{1,0:T(1,128)} %param.41) | copy-start | bytes 1540
  64.1 37.8 %copy-start.24 = (f32[128]{0:T(128)S(1)}, f32[128]{0:T(128)}, u32[]{:S(2)}) copy-start(f32[128]{0:T(128)} %param.30) | copy-start | bytes 1540
  64.1 37.8 %copy-start.14 = (f32[4,128]{1,0:T(4,128)S(1)}, f32[4,128]{1,0:T(4,128)}, u32[]{:S(2)}) copy-start(f32[4,128]{1,0:T(4,128)} %param.27) | copy-start | bytes 6148
  64.1 54.5 %all-to-all-start = ((bf16[8,1024,256]{1,2,0:T(8,128)(2,1)}), bf16[8,1024,256]{1,2,0:T(8,128)(2,1)}, u32[]{:S(2)}, u32[]{:S(2)}) async-start(bf16[8,1024,256]{1,2,0:T(8,128)(2,1)} %broadcast_in_dim.8), calls=%async_computation | async-start | bytes 8388608 | tf_op jit(solution)/shard_map/all_to_all | solution.py:20
  69.0 67.5 %all-gather.5.cloned.1.call-start = ((), (), s32[]{:S(2)}) async-start(), calls=%async_computation.6 | async-start | bytes 1114112 | tf_op jit(solution)/shard_map/all_gather | solution.py:11
  69.9 181.7 %all-gather.7.cloned.1.call-start = ((), (), s32[]{:S(2)}) async-start(), calls=%async_computation.7 | async-start | bytes 6127616 | tf_op jit(solution)/shard_map/all_gather | solution.py:11
  70.8 54.9 %copy-start.10 = (f32[2048]{0:T(1024)S(1)}, f32[2048]{0:T(1024)}, u32[]{:S(2)}) copy-start(f32[2048]{0:T(1024)} %param.22) | copy-start | bytes 24580
  118.6 32.5 %all-to-all-start.3 = ((bf16[128,8,256]{0,2,1:T(8,128)(2,1)}), bf16[128,8,256]{0,2,1:T(8,128)(2,1)S(1)}, u32[]{:S(2)}, u32[]{:S(2)}) async-start(bf16[128,8,256]{0,2,1:T(8,128)(2,1)} %bitcast.16), calls=%async_computation.3 | async-start | bytes 1048576 | tf_op jit(solution)/shard_map/all_to_all | solution.py:133
  140.3 1.4 copy-start.23
  146.2 1.2 copy-start.22
  152.7 31.5 %all-to-all-start.1 = ((bf16[8,1024,128]{1,2,0:T(8,128)(2,1)}), bf16[8,1024,128]{1,2,0:T(8,128)(2,1)S(1)}, u32[]{:S(2)}, u32[]{:S(2)}) async-start(bf16[8,1024,128]{1,2,0:T(8,128)(2,1)} %broadcast_in_dim.9), calls=%async_computation.1 | async-start | bytes 4194304 | tf_op jit(solution)/shard_map/all_to_all | solution.py:20
  185.2 1.3 copy-start.4
  189.9 5.0 %copy-start.7 = (f32[704,128]{1,0:T(8,128)S(1)}, f32[704,128]{1,0:T(8,128)}, u32[]{:S(2)}) copy-start(f32[704,128]{1,0:T(8,128)} %param.40) | copy-start | bytes 1081348
  189.9 6.4 %copy-start.12 = (f32[3,704]{1,0:T(4,128)S(1)}, f32[3,704]{1,0:T(4,128)}, u32[]{:S(2)}) copy-start(f32[3,704]{1,0:T(4,128)} %param.38) | copy-start | bytes 25348
  189.9 6.5 %copy-start.13 = (f32[3,704]{1,0:T(4,128)S(1)}, f32[3,704]{1,0:T(4,128)}, u32[]{:S(2)}) copy-start(f32[3,704]{1,0:T(4,128)} %param.39) | copy-start | bytes 25348
  189.9 54.4 %all-to-all-start.4 = ((bf16[8,1024,256]{1,2,0:T(8,128)(2,1)}), bf16[8,1024,256]{1,2,0:T(8,128)(2,1)}, u32[]{:S(2)}, u32[]{:S(2)}) async-start(bf16[8,1024,256]{1,2,0:T(8,128)(2,1)} %broadcast_in_dim.11), calls=%async_computation.4 | async-start | bytes 8388608 | tf_op jit(solution)/shard_map/all_to_all | solution.py:20
  194.8 52.6 %copy-start.11 = (f32[2048]{0:T(1024)S(1)}, f32[2048]{0:T(1024)}, u32[]{:S(2)}) copy-start(f32[2048]{0:T(1024)} %param.33) | copy-start | bytes 24580
  194.8 127.5 %all-gather.9.cloned.1.call-start = ((), (), s32[]{:S(2)}) async-start(), calls=%async_computation.8 | async-start | bytes 3063808 | tf_op jit(solution)/shard_map/all_gather | solution.py:165
  195.6 175.4 %reduce-scatter.2.cloned.1.call-start = ((), (), s32[]{:S(2)}) async-start(), calls=%async_computation.9 | async-start | bytes 4718592 | tf_op jit(solution)/shard_map/reduce_scatter | solution.py:170
  263.4 11.8 %copy-start.21 = (bf16[2048,1408]{0,1:T(8,128)(2,1)S(1)}, bf16[2048,1408]{0,1:T(8,128)(2,1)}, u32[]{:S(2)}) copy-start(bf16[2048,1408]{0,1:T(8,128)(2,1)} %all-gather.7.cloned.1.call-done) | copy-start | bytes 17301508
  272.8 3.2 copy-start.2
  294.4 27.8 %copy-start.3 = (f32[88,8,2,512]{3,1,2,0:T(8,128)S(1)}, f32[88,8,2,512]{3,1,2,0:T(8,128)}, u32[]{:S(2)}) copy-start(f32[88,8,2,512]{3,1,2,0:T(8,128)} %copy.76) | copy-start | bytes 8650756
  330.4 42.5 %copy-start.1 = (bf16[2,64,64]{2,1,0:T(8,128)(2,1)S(1)}, bf16[2,64,64]{2,1,0:T(8,128)(2,1)}, u32[]{:S(2)}) copy-start(bf16[2,64,64]{2,1,0:T(8,128)(2,1)} %param.28) | copy-start | bytes 49156
Sparse Core Ops, SparseCore 0:
  71.7 64.7 all-gather.4
  138.2 103.9 all-gather.6
  243.9 78.2 all-gather.8
  330.6 40.3 reduce-scatter.1
where the time goes:
time: 381 us; the launch traced here: 379 us
  waiting for transfers between devices  192 us (50%)
  starting transfers between devices  42.2 us (11%)
  other arithmetic  40 us (10%)
  matrix products  31.4 us (8%)
  blocking collectives  30.5 us (8%)
  local copies, waits for them, and re-layouts  29 us (8%)
  between operations  14.3 us (4%)
    all_to_all x4, waiting for transfers between devices, copy_for_each(): lax.all_to_all(jnp.broadcast_to(value[None], (size, *value.shape)), axis,...  119 us
    reduce_scatter x1, waiting for transfers between devices, per_device(): lax.psum_scatter(ffn_terms, 'tp', scatter_dimension=1, tiled=True)  40.5 us
    all_to_all x4, starting transfers between devices, copy_for_each(): lax.all_to_all(jnp.broadcast_to(value[None], (size, *value.shape)), axis,...  38.1 us
    all_gather x1, blocking collectives, side_by_side(): filled, at, outs = (lax.all_gather(both, axis, axis=dim, tiled=True), 0, [])  30.5 us
    all_gather x1, waiting for transfers between devices, per_device(): lax.all_gather(down_weight.astype(jnp.bfloat16), 'fs', axis=1, tiled=True)  25.5 us
    add x2, other arithmetic, causal_mix(): totals = totals + padded[:, k:k + seq_len] * filter_taps[k]  19.1 us
    convert_element_type x2, other arithmetic, rms_rows(): return (values * inverse * norm_gain).astype(jnp.bfloat16)  8.31 us
    dot_general x1, matrix products, per_device(): jnp.dot(ffn_hidden, lax.all_gather(down_weight.astype(jnp.bfloat16), 'fs'...  8.18 us
  transfers between devices with their start and end apart: 9, of which 7 were waited for; matrix products, arithmetic and copies ran while one was open for 22% of the time, Pallas kernels for 0%

commit v1 on v0

--- a/solution.py
+++ b/solution.py
@@ -162,7 +162,12 @@
     ffn_terms = (
         jnp.dot(
             ffn_hidden,
-            lax.all_gather(down_weight.astype(jnp.bfloat16), "fs", axis=1, tiled=True),
+            jnp.concatenate(
+                lax.all_to_all(
+                    jnp.stack([down_weight.astype(jnp.bfloat16)] * lax.axis_size("fs")), "fs", 0, 0
+                ),
+                axis=1,
+            ),
             preferred_element_type=jnp.float32,
         )
         * down_cols

time: 381 us -> 487 us (1.28)
  waiting for transfers between devices: 192 us -> 321 us
  other arithmetic: 40 us -> 24.4 us
  local copies, waits for them, and re-layouts: 29 us -> 19.9 us
  starting transfers between devices: 42.2 us -> 50.4 us
  matrix products: 31.4 us -> 26.2 us
    all_gather x2, waiting for transfers between devices: 6.67 us -> 160 us  [side_by_side(): filled, at, outs = (lax.all_gather(both, axis, axis=dim, tiled=True), 0, [])]
    all_gather x1 -> x0, waiting for transfers between devices: 25.5 us -> none  [per_device(): lax.all_gather(down_weight.astype(jnp.bfloat16), 'fs', axis=1, tiled=True)]
    add x2 -> x0, other arithmetic: 19.1 us -> none  [causal_mix(): totals = totals + padded[:, k:k + seq_len] * filter_taps[k]]
    all_to_all x0 -> x1, starting transfers between devices: none -> 8.22 us  [per_device(): lax.all_to_all(jnp.stack([down_weight.astype(jnp.bfloat16)] * lax.axis_si...]
    reshape x2 -> x1, local copies, waits for them, and re-layouts: 7.97 us -> 0.87 us  [causal_mix(): grouped = values.reshape(-1, seq_len, columns)]
    unnamed x54 -> x50, local copies, waits for them, and re-layouts: 7.7 us -> 2.24 us
  transfers between devices with their start and end apart: 9 -> 9, of which waited for: 7 -> 7; matrix products, arithmetic and copies ran while one was open for 22% -> 10% of each run, Pallas kernels for 0% -> 0%
where the time goes in v1:
time: 487 us; the launch traced here: 486 us
  waiting for transfers between devices  321 us (66%)
  starting transfers between devices  50.4 us (10%)
  blocking collectives  30.5 us (6%)
  matrix products  26.2 us (5%)
  other arithmetic  24.4 us (5%)
  local copies, waits for them, and re-layouts  19.9 us (4%)
  between operations  14.3 us (3%)
    all_gather x2, waiting for transfers between devices, side_by_side(): filled, at, outs = (lax.all_gather(both, axis, axis=dim, tiled=True), 0, [])  160 us
    all_to_all x4, waiting for transfers between devices, copy_for_each(): lax.all_to_all(jnp.broadcast_to(value[None], (size, *value.shape)), axis,...  121 us
    reduce_scatter x1, waiting for transfers between devices, per_device(): lax.psum_scatter(ffn_terms, 'tp', scatter_dimension=1, tiled=True)  40.2 us
    all_to_all x4, starting transfers between devices, copy_for_each(): lax.all_to_all(jnp.broadcast_to(value[None], (size, *value.shape)), axis,...  38.1 us
    all_gather x1, blocking collectives, side_by_side(): filled, at, outs = (lax.all_gather(both, axis, axis=dim, tiled=True), 0, [])  30.5 us
  transfers between devices with their start and end apart: 9, of which 7 were waited for; matrix products, arithmetic and copies ran while one was open for 10% of the time, Pallas kernels for 0%

profile of v1, /device:TPU:40, one launch (start us, length us, event | category | flops | bytes accessed | tf_op | source)
XLA Modules:
  0.0 486.3 jit_solution(511642881625622364)
XLA Ops:
  6.6 0.9 convert_element_type.154
  7.5 0.9 broadcast_in_dim.10
  8.4 24.0 %all-to-all-start.2 = ((bf16[16,128,128]{1,2,0:T(8,128)(2,1)}), bf16[16,128,128]{1,2,0:T(8,128)(2,1)}, u32[]{:S(2)}, u32[]{:S(2)}) async-start(bf16[16,128,128]{1,2,0:T(8,128)(2,1)} %broadcast_in_dim.10), calls=%async_computation.2 | async-start | bytes 1048576 | tf_op jit(solution)/shard_map/all_to_all | solution.py:20
  32.4 1.2 copy.98
  33.7 27.8 %all-to-all-done.2 = bf16[16,128,128]{1,2,0:T(8,128)(2,1)} async-done(((bf16[16,128,128]{1,2,0:T(8,128)(2,1)}), bf16[16,128,128]{1,2,0:T(8,128)(2,1)}, u32[]{:S(2)}, u32[]{:S(2)}) %all-to-all-start.2) | async-done | bytes 524320 | tf_op jit(solution)/shard_map/all_to_all | solution.py:20
  61.4 2.6 broadcast_in_dim.8
  64.1 4.9 %all-to-all-start = ((bf16[8,1024,256]{1,2,0:T(8,128)(2,1)}), bf16[8,1024,256]{1,2,0:T(8,128)(2,1)}, u32[]{:S(2)}, u32[]{:S(2)}) async-start(bf16[8,1024,256]{1,2,0:T(8,128)(2,1)} %broadcast_in_dim.8), calls=%async_computation | async-start | bytes 8388608 | tf_op jit(solution)/shard_map/all_to_all | solution.py:20
  69.1 0.6 pad_maximum_fusion.3
  69.9 30.5 %all-gather = f32[16,1,360]{2,1,0:T(1,128)S(1)} all-gather(f32[1,1,360]{2,1,0:T(1,128)S(1)} %bitcast.158), channel_id=1, replica_groups=mesh['grp'=2,'fs'=16,'tp'=8] {'fs'}, dimensions={0}, use_global_device_ids=true | all-gather | bytes 24480 | tf_op jit(solution)/shard_map/all_gather | solution.py:11
  100.9 17.6 %all-to-all-done = bf16[8,1024,256]{1,2,0:T(8,128)(2,1)} async-done(((bf16[8,1024,256]{1,2,0:T(8,128)(2,1)}), bf16[8,1024,256]{1,2,0:T(8,128)(2,1)}, u32[]{:S(2)}, u32[]{:S(2)}) %all-to-all-start) | async-done | bytes 4194336 | tf_op jit(solution)/shard_map/all_to_all | solution.py:20
  118.5 3.9 all-to-all-start.3
  122.4 3.1 multiply_reduce_fusion.1
  125.6 4.2 fusion.3
  129.7 6.6 %all-gather.4.cloned.1.call-done = bf16[2048,256]{1,0:T(8,128)(2,1)} async-done(((bf16[128,256]{1,0:T(8,128)(2,1)}), bf16[2048,256]{1,0:T(8,128)(2,1)}) %all-gather.4.cloned.1.call-update) | async-done | bytes 1048592 | tf_op jit(solution)/shard_map/all_gather | solution.py:11
  136.4 3.6 convolution_multiply_fusion.9
  140.6 0.3 fusion.59
  141.0 0.4 div.28
  141.6 0.3 fusion.55
  142.0 0.4 div.30
  142.7 0.6 multiply_exponential_fusion
  146.5 0.8 copy-done.21
  147.3 3.5 fusion.68
  150.9 1.6 broadcast_in_dim.9
  152.6 4.4 all-to-all-start.1
  157.3 26.8 %all-to-all-done.1 = bf16[8,1024,128]{1,2,0:T(8,128)(2,1)S(1)} async-done(((bf16[8,1024,128]{1,2,0:T(8,128)(2,1)}), bf16[8,1024,128]{1,2,0:T(8,128)(2,1)S(1)}, u32[]{:S(2)}, u32[]{:S(2)}) %all-to-all-start.1) | async-done | bytes 2097184 | tf_op jit(solution)/shard_map/all_to_all | solution.py:20
  184.1 0.3 fusion.38
  184.4 0.3 fusion.40
  184.8 0.3 fusion.42
  185.1 0.3 fusion.44
  185.4 0.3 fusion.46
  186.4 0.6 fusion.51
  187.2 2.6 broadcast_in_dim.11
  189.9 4.9 %all-to-all-start.4 = ((bf16[8,1024,256]{1,2,0:T(8,128)(2,1)}), bf16[8,1024,256]{1,2,0:T(8,128)(2,1)}, u32[]{:S(2)}, u32[]{:S(2)}) async-start(bf16[8,1024,256]{1,2,0:T(8,128)(2,1)} %broadcast_in_dim.11), calls=%async_computation.4 | async-start | bytes 8388608 | tf_op jit(solution)/shard_map/all_to_all | solution.py:20
  194.9 0.8 pad_maximum_fusion
  195.7 48.5 %all-to-all-done.4 = bf16[8,1024,256]{1,2,0:T(8,128)(2,1)} async-done(((bf16[8,1024,256]{1,2,0:T(8,128)(2,1)}), bf16[8,1024,256]{1,2,0:T(8,128)(2,1)}, u32[]{:S(2)}, u32[]{:S(2)}) %all-to-all-start.4) | async-done | bytes 4194336 | tf_op jit(solution)/shard_map/all_to_all | solution.py:20
  244.3 2.1 stack.2
  246.3 8.2 %all-to-all-start.5 = ((bf16[16,704,128]{2,1,0:T(8,128)(2,1)}), bf16[16,704,128]{2,1,0:T(8,128)(2,1)S(1)}, u32[]{:S(2)}, u32[]{:S(2)}) async-start(bf16[16,704,128]{2,1,0:T(8,128)(2,1)} %stack.2), calls=%async_computation.5 | async-start | bytes 5767168 | tf_op jit(solution)/shard_map/all_to_all | solution.py:166
  255.3 3.1 multiply_reduce_fusion
  258.5 4.2 fusion.1
  262.6 152.9 %all-gather.6.cloned.1.call-done = bf16[2048,1408]{0,1:T(8,128)(2,1)} async-done(((bf16[128,1408]{0,1:T(8,128)(2,1)}), bf16[2048,1408]{0,1:T(8,128)(2,1)}) %all-gather.6.cloned.1.call-update) | async-done | bytes 5767184 | tf_op jit(solution)/shard_map/all_gather | solution.py:11
  415.5 5.9 %fusion.20 = f32[1024,704]{0,1:T(8,128)S(1)} fusion(bf16[1024,2048]{0,1:T(8,128)(2,1)} %fusion.1, bf16[2048,1408]{0,1:T(8,128)(2,1)} %all-gather.6.cloned.1.call-done, f32[704]{0:T(1024)S(1)} %mul.463), kind=kOutput, calls=%fused_computation.31 | convolution fusion | flops 2953510912 | bytes 9964288 | tf_op jit(solution)/shard_map/dot_general | solution.py:154
  421.5 3.2 fusion.23
  424.7 0.9 copy_bitcast_fusion
  425.6 4.1 fusion.26
  429.7 1.4 copy.132
  431.1 6.4 %multiply_convert_fusion = bf16[1024,2048]{1,0:T(8,128)(2,1)} fusion(bf16[1024,704]{0,1:T(8,128)(2,1)} %bitcast.143, f32[2048]{0:T(1024)S(1)} %mul.489, bf16[16,704,128]{2,1,0:T(8,128)(2,1)S(1)} %all-to-all-done.5), kind=kOutput, calls=%fused_computation.6 | convolution fusion | flops 2956984320 | bytes 8527872 | tf_op jit(solution)/shard_map/dot_general | solution.py:163
  437.6 40.2 %reduce-scatter.2.cloned.1.call-done = bf16[1024,256]{1,0:T(8,128)(2,1)} async-done(((bf16[1024,2048]{1,0:T(8,128)(2,1)}), bf16[1024,256]{1,0:T(8,128)(2,1)}) %reduce-scatter.2.cloned.1.call-update) | async-done | bytes 524304 | tf_op jit(solution)/shard_map/reduce_scatter | solution.py:175
  477.8 2.0 add_convert_fusion
  (196 shorter events, 6.8 us)
Async XLA Ops:
  6.5 134.0 %copy-start = (bf16[2,64,64]{2,1,0:T(8,128)(2,1)S(1)}, bf16[2,64,64]{2,1,0:T(8,128)(2,1)}, u32[]{:S(2)}) copy-start(bf16[2,64,64]{2,1,0:T(8,128)(2,1)} %param.28) | copy-start | bytes 49156
  8.4 53.0 %all-to-all-start.2 = ((bf16[16,128,128]{1,2,0:T(8,128)(2,1)}), bf16[16,128,128]{1,2,0:T(8,128)(2,1)}, u32[]{:S(2)}, u32[]{:S(2)}) async-start(bf16[16,128,128]{1,2,0:T(8,128)(2,1)} %broadcast_in_dim.10), calls=%async_computation.2 | async-start | bytes 1048576 | tf_op jit(solution)/shard_map/all_to_all | solution.py:20
  64.0 5.1 %copy-start.7 = (f32[128,128]{1,0:T(8,128)S(1)}, f32[128,128]{1,0:T(8,128)}, u32[]{:S(2)}) copy-start(f32[128,128]{1,0:T(8,128)} %param.23) | copy-start | bytes 196612
  64.0 5.1 %copy-start.8 = (f32[128,128]{1,0:T(8,128)S(1)}, f32[128,128]{1,0:T(8,128)}, u32[]{:S(2)}) copy-start(f32[128,128]{1,0:T(8,128)} %param.24) | copy-start | bytes 196612
  64.0 5.8 %copy-start.14 = (f32[1,8]{1,0:T(1,128)S(1)}, f32[1,8]{1,0:T(1,128)}, u32[]{:S(2)}) copy-start(f32[1,8]{1,0:T(1,128)} %param.25) | copy-start | bytes 100
  64.0 5.8 %copy-start.15 = (f32[1,8]{1,0:T(1,128)S(1)}, f32[1,8]{1,0:T(1,128)}, u32[]{:S(2)}) copy-start(f32[1,8]{1,0:T(1,128)} %param.26) | copy-start | bytes 100
  64.0 5.8 %copy-start.16 = (f32[1,128]{1,0:T(1,128)S(1)}, f32[1,128]{1,0:T(1,128)}, u32[]{:S(2)}) copy-start(f32[1,128]{1,0:T(1,128)} %param.32) | copy-start | bytes 1540
  64.0 5.8 %copy-start.17 = (f32[1,44]{1,0:T(1,128)S(1)}, f32[1,44]{1,0:T(1,128)}, u32[]{:S(2)}) copy-start(f32[1,44]{1,0:T(1,128)} %param.36) | copy-start | bytes 532
  64.0 5.8 %copy-start.18 = (f32[1,44]{1,0:T(1,128)S(1)}, f32[1,44]{1,0:T(1,128)}, u32[]{:S(2)}) copy-start(f32[1,44]{1,0:T(1,128)} %param.37) | copy-start | bytes 532
  64.0 5.8 %copy-start.19 = (f32[1,128]{1,0:T(1,128)S(1)}, f32[1,128]{1,0:T(1,128)}, u32[]{:S(2)}) copy-start(f32[1,128]{1,0:T(1,128)} %param.41) | copy-start | bytes 1540
  64.0 36.8 %copy-start.23 = (f32[128]{0:T(128)S(1)}, f32[128]{0:T(128)}, u32[]{:S(2)}) copy-start(f32[128]{0:T(128)} %param.30) | copy-start | bytes 1540
  64.1 36.8 %copy-start.13 = (f32[4,128]{1,0:T(4,128)S(1)}, f32[4,128]{1,0:T(4,128)}, u32[]{:S(2)}) copy-start(f32[4,128]{1,0:T(4,128)} %param.27) | copy-start | bytes 6148
  64.1 54.5 %all-to-all-start = ((bf16[8,1024,256]{1,2,0:T(8,128)(2,1)}), bf16[8,1024,256]{1,2,0:T(8,128)(2,1)}, u32[]{:S(2)}, u32[]{:S(2)}) async-start(bf16[8,1024,256]{1,2,0:T(8,128)(2,1)} %broadcast_in_dim.8), calls=%async_computation | async-start | bytes 8388608 | tf_op jit(solution)/shard_map/all_to_all | solution.py:20
  68.9 56.6 %copy-start.9 = (f32[2048]{0:T(1024)S(1)}, f32[2048]{0:T(1024)}, u32[]{:S(2)}) copy-start(f32[2048]{0:T(1024)} %param.22) | copy-start | bytes 24580
  69.0 67.4 %all-gather.4.cloned.1.call-start = ((), (), s32[]{:S(2)}) async-start(), calls=%async_computation.7 | async-start | bytes 1114112 | tf_op jit(solution)/shard_map/all_gather | solution.py:11
  118.5 32.4 %all-to-all-start.3 = ((bf16[128,8,256]{0,2,1:T(8,128)(2,1)}), bf16[128,8,256]{0,2,1:T(8,128)(2,1)S(1)}, u32[]{:S(2)}, u32[]{:S(2)}) async-start(bf16[128,8,256]{0,2,1:T(8,128)(2,1)} %bitcast.16), calls=%async_computation.3 | async-start | bytes 1048576 | tf_op jit(solution)/shard_map/all_to_all | solution.py:133
  140.2 1.4 copy-start.22
  146.0 1.2 copy-start.21
  152.6 31.5 %all-to-all-start.1 = ((bf16[8,1024,128]{1,2,0:T(8,128)(2,1)}), bf16[8,1024,128]{1,2,0:T(8,128)(2,1)S(1)}, u32[]{:S(2)}, u32[]{:S(2)}) async-start(bf16[8,1024,128]{1,2,0:T(8,128)(2,1)} %broadcast_in_dim.9), calls=%async_computation.1 | async-start | bytes 4194304 | tf_op jit(solution)/shard_map/all_to_all | solution.py:20
  185.1 1.3 copy-start.3
  189.8 5.0 %copy-start.4 = (f32[128,704]{0,1:T(8,128)S(1)}, f32[128,704]{0,1:T(8,128)}, u32[]{:S(2)}) copy-start(f32[128,704]{0,1:T(8,128)} %param.34) | copy-start | bytes 1081348
  189.8 5.0 %copy-start.5 = (f32[128,704]{0,1:T(8,128)S(1)}, f32[128,704]{0,1:T(8,128)}, u32[]{:S(2)}) copy-start(f32[128,704]{0,1:T(8,128)} %param.35) | copy-start | bytes 1081348
  189.9 5.9 %copy-start.6 = (f32[704,128]{1,0:T(8,128)S(1)}, f32[704,128]{1,0:T(8,128)}, u32[]{:S(2)}) copy-start(f32[704,128]{1,0:T(8,128)} %param.40) | copy-start | bytes 1081348
  189.9 54.4 %all-to-all-start.4 = ((bf16[8,1024,256]{1,2,0:T(8,128)(2,1)}), bf16[8,1024,256]{1,2,0:T(8,128)(2,1)}, u32[]{:S(2)}, u32[]{:S(2)}) async-start(bf16[8,1024,256]{1,2,0:T(8,128)(2,1)} %broadcast_in_dim.11), calls=%async_computation.4 | async-start | bytes 8388608 | tf_op jit(solution)/shard_map/all_to_all | solution.py:20
  194.7 220.8 %all-gather.6.cloned.1.call-start = ((), (), s32[]{:S(2)}) async-start(), calls=%async_computation.8 | async-start | bytes 6127616 | tf_op jit(solution)/shard_map/all_gather | solution.py:11
  246.3 8.9 %copy-start.11 = (f32[3,704]{1,0:T(4,128)S(1)}, f32[3,704]{1,0:T(4,128)}, u32[]{:S(2)}) copy-start(f32[3,704]{1,0:T(4,128)} %param.39) | copy-start | bytes 25348
  246.3 8.9 %copy-start.12 = (f32[3,704]{1,0:T(4,128)S(1)}, f32[3,704]{1,0:T(4,128)}, u32[]{:S(2)}) copy-start(f32[3,704]{1,0:T(4,128)} %param.38) | copy-start | bytes 25348
  246.3 184.8 %all-to-all-start.5 = ((bf16[16,704,128]{2,1,0:T(8,128)(2,1)}), bf16[16,704,128]{2,1,0:T(8,128)(2,1)S(1)}, u32[]{:S(2)}, u32[]{:S(2)}) async-start(bf16[16,704,128]{2,1,0:T(8,128)(2,1)} %stack.2), calls=%async_computation.5 | async-start | bytes 5767168 | tf_op jit(solution)/shard_map/all_to_all | solution.py:166
  254.6 3.9 copy-start.10
  254.6 223.2 %reduce-scatter.2.cloned.1.call-start = ((), (), s32[]{:S(2)}) async-start(), calls=%async_computation.9 | async-start | bytes 4718592 | tf_op jit(solution)/shard_map/reduce_scatter | solution.py:175
  415.5 5.9 %copy-start.2 = (bf16[1024,2048]{0,1:T(8,128)(2,1)S(1)}, bf16[1024,2048]{0,1:T(8,128)(2,1)}, u32[]{:S(2)}) copy-start(bf16[1024,2048]{0,1:T(8,128)(2,1)} %fusion.1) | copy-start | bytes 12582916
  415.5 6.0 %copy-start.20 = (bf16[2048,1408]{0,1:T(8,128)(2,1)S(1)}, bf16[2048,1408]{0,1:T(8,128)(2,1)}, u32[]{:S(2)}) copy-start(bf16[2048,1408]{0,1:T(8,128)(2,1)} %all-gather.6.cloned.1.call-done) | copy-start | bytes 17301508
  437.5 42.2 %copy-start.1 = (bf16[2,64,64]{2,1,0:T(8,128)(2,1)S(1)}, bf16[2,64,64]{2,1,0:T(8,128)(2,1)}, u32[]{:S(2)}) copy-start(bf16[2,64,64]{2,1,0:T(8,128)(2,1)} %param.28) | copy-start | bytes 49156
Sparse Core Ops, SparseCore 0:
  71.6 64.7 all-gather.3
  197.3 218.1 all-gather.5
  437.7 40.0 reduce-scatter.1
